TPU v7x, 32 devices: a whole 2x2x4 slice. The times are simulated.
32 devices in a mesh: rep: 2 (over x), fs: 4 (over z), tp: 4 (over y, core).
Axes of the slice: x: 2, y: 2, z: 4, core: 2. Of those that a mesh axis runs over, the one named last changes fastest.
Arguments:
- tokens: bfloat16 [4096, 1024], P(('rep', 'fs', 'tp')), may hold values from -6 to 6
- w_up: bfloat16 [1024, 4096], P('fs', 'tp'), may hold values from -0.1875 to 0.1875
- w_down: bfloat16 [4096, 1024], P('tp', 'fs'), may hold values from -0.09375 to 0.09375
- out_gain: float32 [1024], replicated, may hold values from 0.1 to 1.9
- out_shift: float32 [1024], replicated, may hold values from -3 to 3
Outputs:
- normed: bfloat16 [4096, 1024], P(('rep', 'fs', 'tp'))
All inputs are finite; a program needn't handle non-finite values.
Results may differ from a plain program's by a relative error of at most 0.015.
Values may be sent and summed in bfloat16 or wider, within the bound.
A program may use at most 64 MiB of HBM per device.

v0:
```python
import jax
import jax.numpy as jnp
from jax import lax
from jax.sharding import PartitionSpec as P

residual_scale = 2.0**0.25
norm_eps = 1e-05


def over_all(share, axis, dim, apply):
    everything = lax.all_gather(share, axis, axis=dim, tiled=True)
    return apply(everything, jnp.int32(0))


def summed_rows(product, extent, axis):
    whole = product(jnp.int32(0), extent * lax.axis_size(axis)).astype(jnp.bfloat16)
    return lax.psum_scatter(whole, axis, scatter_dimension=0, tiled=True).astype(jnp.float32)


def layer_norm(summed, out_gain, out_shift):
    row_mean = jnp.mean(summed, axis=-1, keepdims=True)
    centered = summed - row_mean
    row_var = jnp.mean(centered * centered, axis=-1, keepdims=True)
    return centered * lax.rsqrt(row_var + norm_eps) * out_gain + out_shift


def squared_relu(pre_act):
    return jnp.square(jnp.maximum(pre_act, 0.0)).astype(jnp.bfloat16)


def shards(tokens, w_up, w_down, out_gain, out_shift):
    up_block = lax.all_gather(w_up, "fs", axis=0, tiled=True)

    def activate(block_rows, offset):
        return squared_relu(jnp.dot(block_rows, up_block, preferred_element_type=jnp.float32))

    hidden = over_all(tokens, "tp", 0, activate)
    down_block = lax.all_gather(w_down, "fs", axis=1, tiled=True)
    own_count = tokens.shape[0]

    def project(offset, how_many):
        picked = lax.dynamic_slice_in_dim(hidden, offset, how_many, 0)
        return jnp.dot(picked, down_block, preferred_element_type=jnp.float32)

    branch = summed_rows(project, own_count, "tp")
    summed = residual_scale * tokens.astype(jnp.float32) + branch
    return layer_norm(summed, out_gain, out_shift).astype(jnp.bfloat16)


def solution(mesh):
    in_specs = (P(("rep", "fs", "tp"), None), P("fs", "tp"), P("tp", "fs"), P(), P())
    out_specs = P(("rep", "fs", "tp"), None)
    return jax.shard_map(shards, mesh=mesh, in_specs=in_specs, out_specs=out_specs, check_vma=False)
```

profile of v0, /device:TPU:0, one launch (start us, length us, event | category | flops | bytes accessed | tf_op | source)
XLA Modules:
  0.0 162.0 jit_solution(3515093248988575749)
XLA Ops:
  6.5 0.0 all-gather.4.cloned.1.call-start
  6.5 0.7 all-gather.4.cloned.1.call-update
  7.3 0.0 all-gather.6.cloned.1.call-start
  7.3 0.7 all-gather.6.cloned.1.call-update
  8.0 0.0 all-gather.8.cloned.1.call-start
  8.1 0.7 all-gather.8.cloned.1.call-update
  8.7 0.0 copy-start
  8.8 0.0 reduce-scatter.2.cloned.1.call-start
  8.8 19.6 %all-gather.4.cloned.1.call-done = bf16[512,1024]{1,0:T(8,128)(2,1)} async-done(((bf16[128,1024]{1,0:T(8,128)(2,1)}), bf16[512,1024]{1,0:T(8,128)(2,1)}) %all-gather.4.cloned.1.call-update) | async-done | bytes 1048592 | tf_op jit(solution)/shard_map/all_gather | solution.py:11
  28.3 47.3 %all-gather.6.cloned.1.call-done = bf16[1024,1024]{1,0:T(8,128)(2,1)} async-done(((bf16[256,1024]{1,0:T(8,128)(2,1)}), bf16[1024,1024]{1,0:T(8,128)(2,1)}) %all-gather.6.cloned.1.call-update) | async-done | bytes 2097168 | tf_op jit(solution)/shard_map/all_gather | solution.py:32
  75.6 46.7 %all-gather.8.cloned.1.call-done = bf16[1024,1024]{1,0:T(8,128)(2,1)} async-done(((bf16[1024,256]{1,0:T(8,128)(2,1)}), bf16[1024,1024]{1,0:T(8,128)(2,1)}) %all-gather.8.cloned.1.call-update) | async-done | bytes 2097168 | tf_op jit(solution)/shard_map/all_gather | solution.py:38
  122.3 5.8 %convolution_convert_fusion = bf16[512,1024]{1,0:T(8,128)(2,1)} fusion(bf16[1024,1024]{1,0:T(8,128)(2,1)} %all-gather.8.cloned.1.call-done, bf16[512,1024]{1,0:T(8,128)(2,1)} %all-gather.4.cloned.1.call-done, bf16[1024,1024]{1,0:T(8,128)(2,1)} %all-gather.6.cloned.1.call-done), kind=kOutput, calls=%fused_computation.1 | convolution fusion | flops 2149580800 | bytes 6291456 | tf_op jit(solution)/shard_map/dot_general | solution.py:43
  128.1 0.0 copy-start.1
  128.1 0.0 copy-start.2
  128.1 0.0 reduce-scatter.2.cloned.1.call-update
  128.1 23.2 %reduce-scatter.2.cloned.1.call-done = bf16[128,1024]{1,0:T(8,128)(2,1)} async-done(((bf16[512,1024]{1,0:T(8,128)(2,1)}), bf16[128,1024]{1,0:T(8,128)(2,1)}) %reduce-scatter.2.cloned.1.call-update) | async-done | bytes 262160 | tf_op jit(solution)/shard_map/reduce_scatter | solution.py:17
  151.3 0.0 copy-done
  151.3 1.1 fusion
  152.4 1.2 multiply_reduce_fusion
  153.6 0.0 copy-done.1
  153.6 0.0 copy-done.2
  153.6 1.8 %add_convert_fusion = bf16[128,1024]{1,0:T(8,128)(2,1)} fusion(bf16[128,1024]{1,0:T(8,128)(2,1)} %reduce-scatter.2.cloned.1.call-done, bf16[128,1024]{1,0:T(8,128)(2,1)S(1)} %copy-done, f32[1024]{0:T(1024)S(1)} %copy-done.1, f32[1024]{0:T(1024)S(1)} %copy-done.2, f32[128]{0:T(128)S(1)} %add_rsqrt_fusion, f32[128]{0:T(128)S(1)} %broadcast_multiply_fusion), kind=kLoop, calls=%fused_computation.2 | loop fusion | flops 1179648 | bytes 795648 | tf_op jit(solution)/shard_map/convert_element_type | solution.py:47
  (2 shorter events, 0.0 us)
Async XLA Ops:
  6.5 21.8 %all-gather.4.cloned.1.call-start = ((), (), s32[]{:S(2)}) async-start(), calls=%async_computation.1 | async-start | bytes 1310720 | tf_op jit(solution)/shard_map/all_gather | solution.py:11
  7.3 68.3 %all-gather.6.cloned.1.call-start = ((), (), s32[]{:S(2)}) async-start(), calls=%async_computation.2 | async-start | bytes 2621440 | tf_op jit(solution)/shard_map/all_gather | solution.py:32
  8.0 114.3 %all-gather.8.cloned.1.call-start = ((), (), s32[]{:S(2)}) async-start(), calls=%async_computation.3 | async-start | bytes 2621440 | tf_op jit(solution)/shard_map/all_gather | solution.py:38
  8.7 142.6 %copy-start = (bf16[128,1024]{1,0:T(8,128)(2,1)S(1)}, bf16[128,1024]{1,0:T(8,128)(2,1)}, u32[]{:S(2)}) copy-start(bf16[128,1024]{1,0:T(8,128)(2,1)} %param.5) | copy-start | bytes 786436
  8.8 142.6 %reduce-scatter.2.cloned.1.call-start = ((), (), s32[]{:S(2)}) async-start(), calls=%async_computation.4 | async-start | bytes 1310720 | tf_op jit(solution)/shard_map/reduce_scatter | solution.py:17
  128.1 25.5 %copy-start.1 = (f32[1024]{0:T(1024)S(1)}, f32[1024]{0:T(1024)}, u32[]{:S(2)}) copy-start(f32[1024]{0:T(1024)} %param.9) | copy-start | bytes 12292
  128.1 25.5 %copy-start.2 = (f32[1024]{0:T(1024)S(1)}, f32[1024]{0:T(1024)}, u32[]{:S(2)}) copy-start(f32[1024]{0:T(1024)} %param.8) | copy-start | bytes 12292
Sparse Core Ops, SparseCore 0:
  8.9 19.4 all-gather.3
  29.9 45.6 all-gather.5
  77.2 45.0 all-gather.7
  128.3 22.9 reduce-scatter.1
where the time goes:
time: 162 us
  waiting for transfers between devices  139 us (86%)
  between operations  13.2 us (8%)
  matrix products  5.85 us (4%)
  other arithmetic  4.1 us (3%)
    all_gather x1, waiting for transfers between devices, shards(): up_block = lax.all_gather(w_up, 'fs', axis=0, tiled=True)  47.3 us
    all_gather x1, waiting for transfers between devices, shards(): down_block = lax.all_gather(w_down, 'fs', axis=1, tiled=True)  46.7 us
    reduce_scatter x1, waiting for transfers between devices, summed_rows(): lax.psum_scatter(whole, axis, scatter_dimension=0, tiled=True)  23.2 us
    all_gather x1, waiting for transfers between devices, over_all(): everything = lax.all_gather(share, axis, axis=dim, tiled=True)  19.6 us
    dot_general x1, matrix products, project(): return jnp.dot(picked, down_block, preferred_element_type=jnp.float32)  5.85 us
  transfers between devices with their start and end apart: 4, of which 4 were waited for; matrix products, arithmetic and copies ran while one was open for 0% of the time, Pallas kernels for 0%

commit v1 on v0

--- a/solution.py
+++ b/solution.py
@@ -1,3 +1,4 @@
+import functools
 import jax
 import jax.numpy as jnp
 from jax import lax
@@ -5,6 +6,23 @@
 
 residual_scale = 2.0**0.25
 norm_eps = 1e-05
+
+
+def solve_the_runs(field, dim_at):
+    n_shards = jax.lax.psum(1, "fs")
+    y_new = [None] * n_shards
+    y_new[n_shards - 1] = field
+    chunks = [(d, (d + 1) % n_shards) for d in range(n_shards)]
+    for rr in range(n_shards - 2, -1, -1):
+        y_new[rr] = jax.lax.ppermute(y_new[rr + 1], axis_name="fs", perm=chunks)
+    new = jnp.concatenate(y_new, dim_at)
+    newest = jax.lax.axis_index("fs")
+    all_rows = (newest + 1) * field.shape[dim_at]
+    local_next = jnp.roll(new, all_rows, dim_at)
+    return local_next
+
+
+_make_frame = functools.partial(solve_the_runs, dim_at=0)
 
 
 def over_all(share, axis, dim, apply):
@@ -29,7 +47,7 @@
 
 
 def shards(tokens, w_up, w_down, out_gain, out_shift):
-    up_block = lax.all_gather(w_up, "fs", axis=0, tiled=True)
+    up_block = _make_frame(w_up)
 
     def activate(block_rows, offset):
         return squared_relu(jnp.dot(block_rows, up_block, preferred_element_type=jnp.float32))

time: 162 us -> 127 us (0.78)
  waiting for transfers between devices: 139 us -> 94.1 us
  local copies, waits for them, and re-layouts: 0.01 us -> 6.65 us
  starting transfers between devices: 0.12 us -> 3.19 us
    ppermute x0 -> x3, waiting for transfers between devices: none -> 56 us  [solve_the_runs(): y_new[rr] = jax.lax.ppermute(y_new[rr + 1], axis_name='fs', perm=chunks)]
    all_gather x1 -> x0, waiting for transfers between devices: 47.3 us -> none  [shards(): up_block = lax.all_gather(w_up, 'fs', axis=0, tiled=True)]
    all_gather x1, waiting for transfers between devices: 46.7 us -> 13.6 us  [shards(): down_block = lax.all_gather(w_down, 'fs', axis=1, tiled=True)]
    all_gather x1, waiting for transfers between devices: 19.6 us -> 0.01 us  [over_all(): everything = lax.all_gather(share, axis, axis=dim, tiled=True)]
    unnamed x6 -> x15, local copies, waits for them, and re-layouts: 0.01 us -> 5.83 us
    ppermute x0 -> x3, starting transfers between devices: none -> 3.11 us  [solve_the_runs(): y_new[rr] = jax.lax.ppermute(y_new[rr + 1], axis_name='fs', perm=chunks)]
  transfers between devices with their start and end apart: 4 -> 6, of which waited for: 4 -> 5; matrix products, arithmetic and copies ran while one was open for 0% -> 5% of each run, Pallas kernels for 0% -> 0%
where the time goes in v1:
time: 127 us
  waiting for transfers between devices  94.1 us (74%)
  between operations  13.1 us (10%)
  local copies, waits for them, and re-layouts  6.65 us (5%)
  matrix products  5.94 us (5%)
  other arithmetic  4.1 us (3%)
  starting transfers between devices  3.19 us (3%)
    ppermute x3, waiting for transfers between devices, solve_the_runs(): y_new[rr] = jax.lax.ppermute(y_new[rr + 1], axis_name='fs', perm=chunks)  56 us
    reduce_scatter x1, waiting for transfers between devices, summed_rows(): lax.psum_scatter(whole, axis, scatter_dimension=0, tiled=True)  23.1 us
    all_gather x1, waiting for transfers between devices, shards(): down_block = lax.all_gather(w_down, 'fs', axis=1, tiled=True)  13.6 us
    dot_general x1, matrix products, project(): return jnp.dot(picked, down_block, preferred_element_type=jnp.float32)  5.94 us
    unnamed x15, local copies, waits for them, and re-layouts  5.83 us
    ppermute x3, starting transfers between devices, solve_the_runs(): y_new[rr] = jax.lax.ppermute(y_new[rr + 1], axis_name='fs', perm=chunks)  3.11 us
  transfers between devices with their start and end apart: 6, of which 5 were waited for; matrix products, arithmetic and copies ran while one was open for 5% of the time, Pallas kernels for 0%

profile of v1, /device:TPU:0, one launch (start us, length us, event | category | flops | bytes accessed | tf_op | source)
XLA Modules:
  0.0 127.1 jit_solution(9876476326070030130)
XLA Ops:
  6.5 0.0 copy-start.1
  6.5 0.0 all-gather.3.cloned.1.call-start
  6.5 0.7 all-gather.3.cloned.1.call-update
  7.3 0.0 all-gather.5.cloned.1.call-start
  7.3 0.7 all-gather.5.cloned.1.call-update
  8.0 0.0 reduce-scatter.2.cloned.1.call-start
  8.1 3.1 %collective-permute-start = (bf16[256,1024]{1,0:T(8,128)(2,1)}, bf16[256,1024]{1,0:T(8,128)(2,1)S(1)}, u32[]{:S(2)}, u32[]{:S(2)}) collective-permute-start(bf16[256,1024]{1,0:T(8,128)(2,1)} %param.6), channel_id=1, source_target_pairs={{0,4},{4,8},{8,12},{12,0},{1,5},{5,9},{9,13},{13,1},{2,6},{6,10},{... | collective-permute-start | bytes 1572872 | tf_op jit(solution)/shard_map/ppermute | solution.py:17
  11.2 14.2 %collective-permute-done = bf16[256,1024]{1,0:T(8,128)(2,1)S(1)} collective-permute-done((bf16[256,1024]{1,0:T(8,128)(2,1)}, bf16[256,1024]{1,0:T(8,128)(2,1)S(1)}, u32[]{:S(2)}, u32[]{:S(2)}) %collective-permute-start) | collective-permute-done | bytes 524320 | tf_op jit(solution)/shard_map/ppermute | solution.py:17
  25.3 0.0 collective-permute-start.1
  25.3 14.9 %collective-permute-done.1 = bf16[256,1024]{1,0:T(8,128)(2,1)S(1)} collective-permute-done((bf16[256,1024]{1,0:T(8,128)(2,1)S(1)}, bf16[256,1024]{1,0:T(8,128)(2,1)S(1)}, u32[]{:S(2)}, u32[]{:S(2)}) %collective-permute-start.1) | collective-permute-done | bytes 524320 | tf_op jit(solution)/shard_map/ppermute | solution.py:17
  40.2 0.0 collective-permute-start.2
  40.2 26.9 %collective-permute-done.2 = bf16[256,1024]{1,0:T(8,128)(2,1)S(1)} collective-permute-done((bf16[256,1024]{1,0:T(8,128)(2,1)S(1)}, bf16[256,1024]{1,0:T(8,128)(2,1)S(1)}, u32[]{:S(2)}, u32[]{:S(2)}) %collective-permute-start.2) | collective-permute-done | bytes 524320 | tf_op jit(solution)/shard_map/ppermute | solution.py:17
  67.1 0.8 constant_dynamic-update-slice_fusion.7
  68.0 0.8 constant_dynamic-update-slice_fusion.6
  68.8 0.8 constant_dynamic-update-slice_fusion.5
  69.6 0.0 copy-done.1
  69.6 0.8 constant_dynamic-update-slice_fusion.4
  70.5 0.8 constant_dynamic-update-slice_fusion.3
  71.3 0.8 constant_dynamic-update-slice_fusion.2
  72.1 0.8 constant_dynamic-update-slice_fusion.1
  73.0 0.8 constant_dynamic-update-slice_fusion
  73.8 0.0 copy-start
  73.8 0.0 copy-start.2
  73.8 0.0 copy-start.3
  73.8 0.0 all-gather.3.cloned.1.call-done
  73.8 13.6 %all-gather.5.cloned.1.call-done = bf16[1024,1024]{1,0:T(8,128)(2,1)} async-done(((bf16[1024,256]{1,0:T(8,128)(2,1)}), bf16[1024,1024]{1,0:T(8,128)(2,1)}) %all-gather.5.cloned.1.call-update) | async-done | bytes 2097168 | tf_op jit(solution)/shard_map/all_gather | solution.py:56
  87.4 5.9 %convolution_convert_fusion = bf16[512,1024]{1,0:T(8,128)(2,1)} fusion(bf16[1024,1024]{1,0:T(8,128)(2,1)} %all-gather.5.cloned.1.call-done, bf16[512,1024]{1,0:T(8,128)(2,1)} %all-gather.3.cloned.1.call-done, bf16[2048,1024]{1,0:T(8,128)(2,1)} %constant_dynamic-update-slice_fusion, s32[]{:T(128)S(6)} %select_n.14), kind=kOutput, calls=%fused_computation.3 | convolution fusion | flops 2149580800 | bytes 6291460 | tf_op jit(solution)/shard_map/dot_general | solution.py:61
  93.4 0.0 reduce-scatter.2.cloned.1.call-update
  93.4 23.1 %reduce-scatter.2.cloned.1.call-done = bf16[128,1024]{1,0:T(8,128)(2,1)} async-done(((bf16[512,1024]{1,0:T(8,128)(2,1)}), bf16[128,1024]{1,0:T(8,128)(2,1)}) %reduce-scatter.2.cloned.1.call-update) | async-done | bytes 262160 | tf_op jit(solution)/shard_map/reduce_scatter | solution.py:35
  116.5 0.0 copy-done
  116.5 1.1 fusion.6
  117.6 1.2 multiply_reduce_fusion
  118.8 0.0 copy-done.2
  118.8 0.0 copy-done.3
  118.8 1.8 %add_convert_fusion = bf16[128,1024]{1,0:T(8,128)(2,1)} fusion(bf16[128,1024]{1,0:T(8,128)(2,1)} %reduce-scatter.2.cloned.1.call-done, bf16[128,1024]{1,0:T(8,128)(2,1)S(1)} %copy-done, f32[1024]{0:T(1024)S(1)} %copy-done.2, f32[1024]{0:T(1024)S(1)} %copy-done.3, f32[128]{0:T(128)S(1)} %add_rsqrt_fusion, f32[128]{0:T(128)S(1)} %broadcast_multiply_fusion), kind=kLoop, calls=%fused_computation.4 | loop fusion | flops 1179648 | bytes 795648 | tf_op jit(solution)/shard_map/convert_element_type | solution.py:65
  (2 shorter events, 0.0 us)
Async XLA Ops:
  6.5 63.1 %copy-start.1 = (bf16[256,1024]{1,0:T(8,128)(2,1)S(1)}, bf16[256,1024]{1,0:T(8,128)(2,1)}, u32[]{:S(2)}) copy-start(bf16[256,1024]{1,0:T(8,128)(2,1)} %param.6) | copy-start | bytes 1572868
  6.5 67.2 %all-gather.3.cloned.1.call-start = ((), (), s32[]{:S(2)}) async-start(), calls=%async_computation.1 | async-start | bytes 1310720 | tf_op jit(solution)/shard_map/all_gather | solution.py:29
  7.3 80.2 %all-gather.5.cloned.1.call-start = ((), (), s32[]{:S(2)}) async-start(), calls=%async_computation.2 | async-start | bytes 2621440 | tf_op jit(solution)/shard_map/all_gather | solution.py:56
  8.0 108.5 %reduce-scatter.2.cloned.1.call-start = ((), (), s32[]{:S(2)}) async-start(), calls=%async_computation.3 | async-start | bytes 1310720 | tf_op jit(solution)/shard_map/reduce_scatter | solution.py:35
  8.1 17.3 %collective-permute-start = (bf16[256,1024]{1,0:T(8,128)(2,1)}, bf16[256,1024]{1,0:T(8,128)(2,1)S(1)}, u32[]{:S(2)}, u32[]{:S(2)}) collective-permute-start(bf16[256,1024]{1,0:T(8,128)(2,1)} %param.6), channel_id=1, source_target_pairs={{0,4},{4,8},{8,12},{12,0},{1,5},{5,9},{9,13},{13,1},{2,6},{6,10},{... | collective-permute-start | bytes 1572872 | tf_op jit(solution)/shard_map/ppermute | solution.py:17
  25.3 14.9 %collective-permute-start.1 = (bf16[256,1024]{1,0:T(8,128)(2,1)S(1)}, bf16[256,1024]{1,0:T(8,128)(2,1)S(1)}, u32[]{:S(2)}, u32[]{:S(2)}) collective-permute-start(bf16[256,1024]{1,0:T(8,128)(2,1)S(1)} %collective-permute-done), channel_id=1, source_target_pairs={{0,4},{4,8},{8,12},{12,0},{1,5},{5,9},{9,13},{13,1},{2,6},{6,10},{... | collective-permute-start | bytes 1572872 | tf_op jit(solution)/shard_map/ppermute | solution.py:17
  40.2 26.9 %collective-permute-start.2 = (bf16[256,1024]{1,0:T(8,128)(2,1)S(1)}, bf16[256,1024]{1,0:T(8,128)(2,1)S(1)}, u32[]{:S(2)}, u32[]{:S(2)}) collective-permute-start(bf16[256,1024]{1,0:T(8,128)(2,1)S(1)} %collective-permute-done.1), channel_id=1, source_target_pairs={{0,4},{4,8},{8,12},{12,0},{1,5},{5,9},{9,13},{13,1},{2,6},{6,10},{... | collective-permute-start | bytes 1572872 | tf_op jit(solution)/shard_map/ppermute | solution.py:17
  73.8 42.7 %copy-start = (bf16[128,1024]{1,0:T(8,128)(2,1)S(1)}, bf16[128,1024]{1,0:T(8,128)(2,1)}, u32[]{:S(2)}) copy-start(bf16[128,1024]{1,0:T(8,128)(2,1)} %param.5) | copy-start | bytes 786436
  73.8 45.0 %copy-start.2 = (f32[1024]{0:T(1024)S(1)}, f32[1024]{0:T(1024)}, u32[]{:S(2)}) copy-start(f32[1024]{0:T(1024)} %param.9) | copy-start | bytes 12292
  73.8 45.0 %copy-start.3 = (f32[1024]{0:T(1024)S(1)}, f32[1024]{0:T(1024)}, u32[]{:S(2)}) copy-start(f32[1024]{0:T(1024)} %param.8) | copy-start | bytes 12292
Sparse Core Ops, SparseCore 0:
  8.9 19.4 all-gather.2
  29.9 57.4 all-gather.4
  93.5 22.9 reduce-scatter.1
